TPU v7x, 32 devices: a whole 2x2x4 slice. The times are simulated.
32 devices in a mesh: sp: 16 (over z, y, x), tp: 2 (over core).
Axes of the slice: x: 2, y: 2, z: 4, core: 2. Of those that a mesh axis runs over, the one named last changes fastest.
Arguments:
- tokens: bfloat16 [4096, 2048], P('sp', 'tp'), may hold values from -6 to 6
- norm_gain: float32 [2048], replicated, may hold values from 0.1 to 1.9
- query_one: bfloat16 [2048, 512], P(None, 'tp'), may hold values from -6 to 6
- key_one: bfloat16 [2048, 512], P(None, 'tp'), may hold values from -1 to 1
- query_two: bfloat16 [2048, 512], P(None, 'tp'), may hold values from -6 to 6
- key_two: bfloat16 [2048, 512], P(None, 'tp'), may hold values from -1 to 1
- value_weight: bfloat16 [2048, 1024], P(None, 'tp'), may hold values from -0.125 to 0.125
- attn_gate_weight: bfloat16 [2048, 1024], P(None, 'tp'), may hold values from -0.125 to 0.125
- conv_outer: bfloat16 [2048, 1024], P(None, 'tp'), may hold values from -0.125 to 0.125
- conv_inner: bfloat16 [2048, 1024], P(None, 'tp'), may hold values from -0.125 to 0.125
- conv_input: bfloat16 [2048, 1024], P(None, 'tp'), may hold values from -0.125 to 0.125
- conv_taps: bfloat16 [3, 1024], P(None, 'tp'), may hold values from -3.5 to 3.5
- head_lambda: float32 [8], P('tp'), may hold values from 0.3 to 0.8
- head_gain: float32 [128], replicated, may hold values from 0.1 to 1.9
- attn_out_weight: bfloat16 [1024, 2048], P('tp'), may hold values from -0.125 to 0.125
- conv_out_weight: bfloat16 [1024, 2048], P('tp'), may hold values from -0.125 to 0.125
Outputs:
- mixed: bfloat16 [4096, 2048], P(('sp', 'tp'))
All inputs are finite; a program needn't handle non-finite values.
Results may differ from a plain program's by a relative error of at most 0.014.
Values may be sent and summed in bfloat16 or wider, within the bound.
A program may use at most 128 MiB of HBM per device.

v0:
```python
import math

import jax
import jax.numpy as jnp
from jax import lax
from jax.sharding import PartitionSpec as P

D = 2048
KEY_DIM = 64
VALUE_DIM = 128


EPSILON = 1e-06


def with_halo(cells, sides, width):
    for axis, dim in sides:
        count = lax.axis_size(axis)
        ends = count - 1
        head = lax.slice_in_dim(cells, 0, width, axis=dim)
        tail = lax.slice_in_dim(cells, cells.shape[dim] - width, cells.shape[dim], axis=dim)
        cells = jnp.concatenate(
            [
                lax.ppermute(tail, axis, [(i, (i + 1) % count) for i in range(ends)]),
                cells,
                lax.ppermute(head, axis, [((i + 1) % count, i) for i in range(ends)]),
            ],
            axis=dim,
        )
    return cells


def block_size(length):
    for size in range(min(length, 2048), 0, -1):
        if length % size == 0:
            return size
    return 1


def sweep(states, pieces, handle):
    length = pieces[0].shape[0]
    size = block_size(length)
    count = length // size
    if count == 1:
        return handle(states, pieces)

    def one_turn(index, current):
        subset = tuple((lax.dynamic_slice_in_dim(piece, index * size, size, 0) for piece in pieces))
        return handle(current, subset)

    return lax.fori_loop(0, count, one_turn, states)


def absorb(state, queries, keys, values):
    peak, totals, accum = state
    factor_scale = 1.0 / math.sqrt(queries.shape[2])
    scores = (
        jnp.einsum("qhd,khd->hqk", queries, keys, preferred_element_type=jnp.float32) * factor_scale
    )
    new_peak = jnp.maximum(peak, jnp.max(scores, axis=2, keepdims=True))
    factor = jnp.exp(peak - new_peak)
    weights = jnp.exp(scores - new_peak)
    totals = totals * factor + jnp.sum(weights, axis=2, keepdims=True)
    accum = accum * factor + jnp.einsum(
        "hqk,khe->hqe", weights.astype(jnp.bfloat16), values, preferred_element_type=jnp.float32
    )
    return (new_peak, totals, accum)


def local(
    tokens,
    norm_gain,
    query_one,
    key_one,
    query_two,
    key_two,
    value_weight,
    attn_gate_weight,
    conv_outer,
    conv_inner,
    conv_input,
    conv_taps,
    head_lambda,
    head_gain,
    attn_out_weight,
    conv_out_weight,
):
    row_count = tokens.shape[0]
    heads_here = head_lambda.shape[0]
    matrices = (
        query_one,
        key_one,
        query_two,
        key_two,
        value_weight,
        attn_gate_weight,
        conv_outer,
        conv_inner,
        conv_input,
    )
    stacked = jnp.concatenate(matrices, axis=1)
    widened = lax.all_gather(tokens, "tp", axis=1, tiled=True).astype(jnp.float32)
    scaled = (widened * norm_gain).astype(jnp.bfloat16)
    running = jnp.dot(scaled, stacked, preferred_element_type=jnp.float32)
    squares = jnp.sum(widened * widened, axis=1, keepdims=True)
    projected = (running * lax.rsqrt(squares / D + EPSILON)).astype(jnp.bfloat16)
    parts_list = []
    offset = 0
    for matrix in matrices:
        parts_list.append(projected[:, offset : offset + matrix.shape[1]])
        offset = offset + matrix.shape[1]
    first_query, first_key, second_query, second_key, values, attn_gate, outer, inner_a, inner_b = (
        parts_list
    )
    queries_a = first_query.reshape(row_count, heads_here, KEY_DIM)
    queries_b = second_query.reshape(row_count, heads_here, KEY_DIM)
    fresh = (
        jnp.full((heads_here, row_count, 1), -1e30, jnp.float32),
        jnp.zeros((heads_here, row_count, 1), jnp.float32),
        jnp.zeros((heads_here, row_count, VALUE_DIM), jnp.float32),
    )

    def split_keys(keys):
        return keys.reshape(keys.shape[0], heads_here, KEY_DIM)

    def split_values(vals):
        return vals.reshape(vals.shape[0], heads_here, VALUE_DIM)

    def handle_first(state, subset):
        return absorb(state, queries_a, split_keys(subset[0]), split_values(subset[1]))

    def handle_second(state, subset):
        return absorb(state, queries_b, split_keys(subset[0]), split_values(subset[1]))

    state_a = sweep(
        fresh,
        (
            lax.all_gather(first_key, "sp", axis=0, tiled=True),
            lax.all_gather(values, "sp", axis=0, tiled=True),
        ),
        handle_first,
    )
    state_b = sweep(
        fresh,
        (
            lax.all_gather(second_key, "sp", axis=0, tiled=True),
            lax.all_gather(values, "sp", axis=0, tiled=True),
        ),
        handle_second,
    )
    diff = state_a[2] / state_a[1] - head_lambda[:, None, None] * (state_b[2] / state_b[1])
    normed = diff * lax.rsqrt(jnp.mean(diff * diff, axis=2, keepdims=True) + EPSILON) * head_gain
    normed = normed.transpose(1, 0, 2).reshape(row_count, heads_here * VALUE_DIM)
    attn_mix = (normed * jax.nn.silu(attn_gate.astype(jnp.float32))).astype(jnp.bfloat16)
    product = (inner_a.astype(jnp.float32) * inner_b.astype(jnp.float32)).astype(jnp.bfloat16)
    padded = with_halo(product, (("sp", 0),), 1).astype(jnp.float32)
    taps = conv_taps.astype(jnp.float32)
    convolved = taps[0] * padded[:-2] + taps[1] * padded[1:-1] + taps[2] * padded[2:]
    conv_mix = (outer.astype(jnp.float32) * convolved).astype(jnp.bfloat16)
    return lax.psum_scatter(
        (
            jnp.dot(attn_mix, attn_out_weight, preferred_element_type=jnp.float32)
            + jnp.dot(conv_mix, conv_out_weight, preferred_element_type=jnp.float32)
        ).astype(jnp.bfloat16),
        "tp",
        scatter_dimension=0,
        tiled=True,
    )


def solution(mesh):
    return jax.shard_map(
        local,
        mesh=mesh,
        in_specs=(
            P("sp", "tp"),
            P(),
            P(None, "tp"),
            P(None, "tp"),
            P(None, "tp"),
            P(None, "tp"),
            P(None, "tp"),
            P(None, "tp"),
            P(None, "tp"),
            P(None, "tp"),
            P(None, "tp"),
            P(None, "tp"),
            P("tp"),
            P(),
            P("tp", None),
            P("tp", None),
        ),
        out_specs=P(("sp", "tp"), None),
        check_vma=False,
    )
```

profile of v0, /device:TPU:0, one launch (start us, length us, event | category | flops | bytes accessed | tf_op | source)
XLA Modules:
  0.0 297.6 jit_solution(14727345691030483329)
XLA Ops:
  6.5 0.7 all-gather.5.cloned.1.call-update
  7.3 0.0 all-gather.9.cloned.1.call-start
  7.3 2.5 constant_dynamic-update-slice_fusion.8
  9.8 2.4 constant_dynamic-update-slice_fusion.7
  12.2 2.5 constant_dynamic-update-slice_fusion.6
  14.7 2.3 constant_dynamic-update-slice_fusion.5
  17.0 1.5 constant_dynamic-update-slice_fusion.4
  18.6 1.5 constant_dynamic-update-slice_fusion.3
  20.1 1.5 constant_dynamic-update-slice_fusion.2
  21.6 1.5 constant_dynamic-update-slice_fusion.1
  23.1 1.5 constant_dynamic-update-slice_fusion
  24.7 1.5 fusion.27
  26.2 9.5 %fusion.24 = bf16[256,3584]{1,0:T(8,128)(2,1)S(1)} fusion(bf16[2048,3584]{1,0:T(8,128)(2,1)} %constant_dynamic-update-slice_fusion, f32[256]{0:T(256)S(1)} %add_rsqrt_fusion.1, bf16[256,2048]{1,0:T(8,128)(2,1)} %all-gather.5.cloned.1.call-done, f32[2048]{0:T(1024)S(1)} %copy-done.15), kind=kOutput, calls=%fused_computation.37 | convolution fusion | flops 3761504256 | bytes 17572864 | tf_op jit(solution)/shard_map/dot_general | solution.py:104
  35.7 1.3 copy-done.12
  36.9 0.7 slice.70
  37.7 0.0 all-gather.11.cloned.1.call-start
  37.7 1.8 fusion.49
  39.6 0.0 all-gather.7.cloned.1.call-start
  39.7 1.1 multiply_convert_fusion
  40.8 1.3 collective-permute-start.1
  42.1 5.5 %collective-permute-start = (bf16[1,512]{1,0:T(2,128)(2,1)S(1)}, bf16[1,512]{1,0:T(2,128)(2,1)S(1)}, u32[]{:S(2)}, u32[]{:S(2)}) collective-permute-start(bf16[1,512]{1,0:T(2,128)(2,1)S(1)} %get-tuple-element.377), channel_id=1, source_target_pairs={{0,2},{2,4},{4,6},{6,8},{8,10},{10,12},{12,14},{14,16},{16,18},{18... | collective-permute-start | bytes 3080 | tf_op jit(solution)/shard_map/ppermute | solution.py:24
  47.7 0.1 copy.31
  47.8 0.1 copy.28
  47.9 0.2 reduce-scatter.2.cloned.1.call-start
  48.1 0.7 collective-permute-done
  48.9 0.9 maximum_convert_fusion
  49.8 66.4 %all-gather.9.cloned.1.call-done = bf16[4096,512]{1,0:T(8,128)(2,1)} async-done(((bf16[256,512]{1,0:T(8,128)(2,1)}), bf16[4096,512]{1,0:T(8,128)(2,1)}) %all-gather.9.cloned.1.call-update) | async-done | bytes 4194320 | tf_op jit(solution)/shard_map/all_gather | solution.py:139
  116.2 6.3 %copy.30 = bf16[4096,512]{0,1:T(8,128)(2,1)} copy(bf16[4096,512]{1,0:T(8,128)(2,1)} %all-gather.9.cloned.1.call-done) | data formatting | bytes 8388608
  122.5 55.4 %all-gather.11.cloned.1.call-done = bf16[4096,256]{1,0:T(8,128)(2,1)} async-done(((bf16[256,256]{1,0:T(8,128)(2,1)}), bf16[4096,256]{1,0:T(8,128)(2,1)}) %all-gather.11.cloned.1.call-update) | async-done | bytes 2097168 | tf_op jit(solution)/shard_map/all_gather | solution.py:146
  178.0 36.5 %while.37 = (s32[]{:T(128)}, f32[4,256,1]{1,0,2:T(4,128)S(1)}, f32[4,256,1]{1,0,2:T(4,128)S(1)}, f32[4,256,128]{2,1,0:T(8,128)}, bf16[4096,256]{1,0:T(8,128)(2,1...) while((s32[]{:T(128)}, f32[4,256,1]{1,0,2:T(4,128)S(1)}, ...), condition=%wide.region_8.0_spmd.clone, body=%wide.region_5.0_spmd.clone.sunk | while | flops 822482944 | bytes 75694344 | solution.py:51
  178.0 2.3 constant_dynamic-slice_fusion.10
  180.3 1.5 copy.49
  181.8 4.6 %bitcast_reduce_fusion.5 = (f32[4,256]{1,0:T(4,128)S(1)}, f32[4,2048,256]{2,1,0:T(8,128)}) fusion(bf16[2048,4,64]{0,2,1:T(8,128)(2,1)S(1)} %bitcast.116, bf16[256,4,64]{0,2,1:T(8,128)(2,1)S(1)} %get-tuple-element.511), kind=kOutput, calls=%fused_computation.19.clone.1 | convolution fusion | flops 272628736 | bytes 9572352 | tf_op jit(solution)/shard_map/while/body/eval_jaxpr/qhd,khd->hqk/dot_general | solution.py:58
  186.3 5.0 %fusion.87 = f32[4,256]{1,0:T(4,128)S(1)} fusion(f32[4,2048,256]{2,1,0:T(8,128)} %get-tuple-element.482, f32[4,256]{1,0:T(4,128)S(1)} %bitcast.120), kind=kLoop, calls=%fused_computation.22.clone.1 | loop fusion | flops 6290432 | bytes 8396800 | tf_op jit(solution)/shard_map/while/body/eval_jaxpr/reduce_sum | solution.py:63
  191.4 1.8 constant_dynamic-slice_fusion.11
  193.3 2.2 fusion.88
  195.5 0.8 copy-done.6
  196.3 2.3 constant_dynamic-slice_fusion.10
  198.6 1.5 copy.49
  200.1 4.6 %bitcast_reduce_fusion.5 = (f32[4,256]{1,0:T(4,128)S(1)}, f32[4,2048,256]{2,1,0:T(8,128)}) fusion(bf16[2048,4,64]{0,2,1:T(8,128)(2,1)S(1)} %bitcast.116, bf16[256,4,64]{0,2,1:T(8,128)(2,1)S(1)} %get-tuple-element.511), kind=kOutput, calls=%fused_computation.19.clone.1 | convolution fusion | flops 272628736 | bytes 9572352 | tf_op jit(solution)/shard_map/while/body/eval_jaxpr/qhd,khd->hqk/dot_general | solution.py:58
  204.7 4.9 %fusion.87 = f32[4,256]{1,0:T(4,128)S(1)} fusion(f32[4,2048,256]{2,1,0:T(8,128)} %get-tuple-element.482, f32[4,256]{1,0:T(4,128)S(1)} %bitcast.120), kind=kLoop, calls=%fused_computation.22.clone.1 | loop fusion | flops 6290432 | bytes 8396800 | tf_op jit(solution)/shard_map/while/body/eval_jaxpr/reduce_sum | solution.py:63
  209.6 1.8 constant_dynamic-slice_fusion.11
  211.4 2.2 fusion.88
  213.7 0.8 copy-done.6
  214.5 25.3 %all-gather.7.cloned.1.call-done = bf16[4096,256]{1,0:T(8,128)(2,1)} async-done(((bf16[256,256]{1,0:T(8,128)(2,1)}), bf16[4096,256]{1,0:T(8,128)(2,1)}) %all-gather.7.cloned.1.call-update) | async-done | bytes 2097168 | tf_op jit(solution)/shard_map/all_gather | solution.py:138
  239.8 36.4 %while.36 = (s32[]{:T(128)}, f32[4,256,1]{1,0,2:T(4,128)S(1)}, f32[4,256,1]{1,0,2:T(4,128)S(1)}, f32[4,256,128]{2,1,0:T(8,128)}, bf16[4096,256]{1,0:T(8,128)(2,1...) while((s32[]{:T(128)}, f32[4,256,1]{1,0,2:T(4,128)S(1)}, ...), condition=%wide.region_4.0_spmd.clone, body=%wide.region_1.0_spmd.clone.sunk | while | flops 822482944 | bytes 75694344 | solution.py:51
  239.8 2.3 constant_dynamic-slice_fusion.8
  242.1 1.5 copy.48
  243.6 4.6 %bitcast_reduce_fusion.4 = (f32[4,256]{1,0:T(4,128)S(1)}, f32[4,2048,256]{2,1,0:T(8,128)}) fusion(bf16[2048,4,64]{0,2,1:T(8,128)(2,1)S(1)} %bitcast.117, bf16[256,4,64]{0,2,1:T(8,128)(2,1)S(1)} %get-tuple-element.544), kind=kOutput, calls=%fused_computation.1.clone.1 | convolution fusion | flops 272628736 | bytes 9572352 | tf_op jit(solution)/shard_map/while/body/eval_jaxpr/qhd,khd->hqk/dot_general | solution.py:58
  248.2 4.9 %fusion.80 = f32[4,256]{1,0:T(4,128)S(1)} fusion(f32[4,2048,256]{2,1,0:T(8,128)} %get-tuple-element.471, f32[4,256]{1,0:T(4,128)S(1)} %bitcast.122), kind=kLoop, calls=%fused_computation.4.clone.1 | loop fusion | flops 6290432 | bytes 8396800 | tf_op jit(solution)/shard_map/while/body/eval_jaxpr/reduce_sum | solution.py:63
  253.1 1.8 constant_dynamic-slice_fusion.9
  255.0 2.2 fusion.81
  257.2 0.8 copy-done.4
  258.0 2.3 constant_dynamic-slice_fusion.8
  260.3 1.5 copy.48
  261.8 4.6 %bitcast_reduce_fusion.4 = (f32[4,256]{1,0:T(4,128)S(1)}, f32[4,2048,256]{2,1,0:T(8,128)}) fusion(bf16[2048,4,64]{0,2,1:T(8,128)(2,1)S(1)} %bitcast.117, bf16[256,4,64]{0,2,1:T(8,128)(2,1)S(1)} %get-tuple-element.544), kind=kOutput, calls=%fused_computation.1.clone.1 | convolution fusion | flops 272628736 | bytes 9572352 | tf_op jit(solution)/shard_map/while/body/eval_jaxpr/qhd,khd->hqk/dot_general | solution.py:58
  266.4 4.9 %fusion.80 = f32[4,256]{1,0:T(4,128)S(1)} fusion(f32[4,2048,256]{2,1,0:T(8,128)} %get-tuple-element.471, f32[4,256]{1,0:T(4,128)S(1)} %bitcast.122), kind=kLoop, calls=%fused_computation.4.clone.1 | loop fusion | flops 6290432 | bytes 8396800 | tf_op jit(solution)/shard_map/while/body/eval_jaxpr/reduce_sum | solution.py:63
  271.3 1.8 constant_dynamic-slice_fusion.9
  273.2 2.2 fusion.81
  275.4 0.8 copy-done.4
  276.2 1.7 multiply_reduce_fusion
  278.0 1.7 fusion.39
  279.7 4.0 %fusion.25 = bf16[256,2048]{1,0:T(8,128)(2,1)} fusion(f32[256,2048]{1,0:T(8,128)S(1)} %fusion.39, bf16[512,2048]{1,0:T(8,128)(2,1)} %param.35, f32[258,512]{1,0:T(8,128)} %maximum_convert_fusion, bf16[256,3584]{1,0:T(8,128)(2,1)} %copy-done.12, f32[512]{0:T(512)S(1)} %bitcast.128, f32[512]{0:T(512)S(1)} %bitcast.127, f32[512]{0:T(512)S(1)} %bitcast.126), kind=kOutput, calls=%fused_computation.41 | convolution fusion | flops 538968064 | bytes 7084032 | tf_op jit(solution)/shard_map/dot_general | solution.py:163
  283.8 7.3 %reduce-scatter.2.cloned.1.call-done = bf16[128,2048]{1,0:T(8,128)(2,1)} async-done(((bf16[256,2048]{1,0:T(8,128)(2,1)}), bf16[128,2048]{1,0:T(8,128)(2,1)}) %reduce-scatter.2.cloned.1.call-update) | async-done | bytes 524304 | tf_op jit(solution)/shard_map/reduce_scatter | solution.py:160
  (70 shorter events, 0.3 us)
Async XLA Ops:
  6.5 271.4 %copy-start = (bf16[512,2048]{1,0:T(8,128)(2,1)S(1)}, bf16[512,2048]{1,0:T(8,128)(2,1)}, u32[]{:S(2)}) copy-start(bf16[512,2048]{1,0:T(8,128)(2,1)} %param.34) | copy-start | bytes 6291460
  6.5 18.1 %all-gather.5.cloned.1.call-start = ((), (), s32[]{:S(2)}) async-start(), calls=%async_computation.1 | async-start | bytes 1572864 | tf_op jit(solution)/shard_map/all_gather | solution.py:102
  7.3 108.9 %all-gather.9.cloned.1.call-start = ((), (), s32[]{:S(2)}) async-start(), calls=%async_computation.3 | async-start | bytes 4456448 | tf_op jit(solution)/shard_map/all_gather | solution.py:139
  7.3 9.7 %copy-start.7 = (bf16[2048,512]{1,0:T(8,128)(2,1)S(1)}, bf16[2048,512]{1,0:T(8,128)(2,1)}, u32[]{:S(2)}) copy-start(bf16[2048,512]{1,0:T(8,128)(2,1)} %param.26) | copy-start | bytes 6291460
  7.3 11.2 %copy-start.8 = (bf16[2048,512]{1,0:T(8,128)(2,1)S(1)}, bf16[2048,512]{1,0:T(8,128)(2,1)}, u32[]{:S(2)}) copy-start(bf16[2048,512]{1,0:T(8,128)(2,1)} %param.27) | copy-start | bytes 6291460
  7.3 12.8 %copy-start.9 = (bf16[2048,512]{1,0:T(8,128)(2,1)S(1)}, bf16[2048,512]{1,0:T(8,128)(2,1)}, u32[]{:S(2)}) copy-start(bf16[2048,512]{1,0:T(8,128)(2,1)} %param.28) | copy-start | bytes 6291460
  12.2 9.4 %copy-start.10 = (bf16[2048,512]{1,0:T(8,128)(2,1)S(1)}, bf16[2048,512]{1,0:T(8,128)(2,1)}, u32[]{:S(2)}) copy-start(bf16[2048,512]{1,0:T(8,128)(2,1)} %param.29) | copy-start | bytes 6291460
  17.0 6.1 %copy-start.11 = (bf16[2048,512]{1,0:T(8,128)(2,1)S(1)}, bf16[2048,512]{1,0:T(8,128)(2,1)}, u32[]{:S(2)}) copy-start(bf16[2048,512]{1,0:T(8,128)(2,1)} %param.30) | copy-start | bytes 6291460
  18.6 7.6 %copy-start.15 = (f32[2048]{0:T(1024)S(1)}, f32[2048]{0:T(1024)}, u32[]{:S(2)}) copy-start(f32[2048]{0:T(1024)} %param.21) | copy-start | bytes 24580
  26.2 21.4 %copy-start.13 = (bf16[3,512]{1,0:T(4,128)(2,1)S(1)}, bf16[3,512]{1,0:T(4,128)(2,1)}, u32[]{:S(2)}) copy-start(bf16[3,512]{1,0:T(4,128)(2,1)} %param.31) | copy-start | bytes 9220
  35.7 1.3 copy-start.12
  37.7 140.3 %all-gather.11.cloned.1.call-start = ((), (), s32[]{:S(2)}) async-start(), calls=%async_computation.4 | async-start | bytes 2228224 | tf_op jit(solution)/shard_map/all_gather | solution.py:146
  39.6 200.2 %all-gather.7.cloned.1.call-start = ((), (), s32[]{:S(2)}) async-start(), calls=%async_computation.2 | async-start | bytes 2228224 | tf_op jit(solution)/shard_map/all_gather | solution.py:138
  40.8 7.4 %collective-permute-start.1 = (bf16[1,512]{1,0:T(2,128)(2,1)S(1)}, bf16[1,512]{1,0:T(2,128)(2,1)S(1)}, u32[]{:S(2)}, u32[]{:S(2)}) collective-permute-start(bf16[1,512]{1,0:T(2,128)(2,1)S(1)} %get-tuple-element.378), channel_id=1, source_target_pairs={{2,0},{4,2},{6,4},{8,6},{10,8},{12,10},{14,12},{16,14},{18,16},{20... | collective-permute-start | bytes 3080 | tf_op jit(solution)/shard_map/ppermute | solution.py:26
  42.1 6.8 %collective-permute-start = (bf16[1,512]{1,0:T(2,128)(2,1)S(1)}, bf16[1,512]{1,0:T(2,128)(2,1)S(1)}, u32[]{:S(2)}, u32[]{:S(2)}) collective-permute-start(bf16[1,512]{1,0:T(2,128)(2,1)S(1)} %get-tuple-element.377), channel_id=1, source_target_pairs={{0,2},{2,4},{4,6},{6,8},{8,10},{10,12},{12,14},{14,16},{16,18},{18... | collective-permute-start | bytes 3080 | tf_op jit(solution)/shard_map/ppermute | solution.py:24
  47.9 243.2 %reduce-scatter.2.cloned.1.call-start = ((), (), s32[]{:S(2)}) async-start(), calls=%async_computation.5 | async-start | bytes 1572864 | tf_op jit(solution)/shard_map/reduce_scatter | solution.py:160
  186.3 6.9 %copy-start.5 = (f32[4,256,128]{2,1,0:T(8,128)S(1)}, f32[4,256,128]{2,1,0:T(8,128)}, u32[]{:S(2)}) copy-start(f32[4,256,128]{2,1,0:T(8,128)} %get-tuple-element.498) | copy-start | bytes 1572868 | tf_op jit(solution)/shard_map/while
  186.3 6.9 %copy-start.1 = (f32[4,2048,256]{2,1,0:T(8,128)S(1)}, f32[4,2048,256]{2,1,0:T(8,128)}, u32[]{:S(2)}) copy-start(f32[4,2048,256]{2,1,0:T(8,128)} %get-tuple-element.482) | copy-start | bytes 25165828 | tf_op jit(solution)/shard_map/while
  195.5 0.8 copy-start.6
  204.6 6.8 %copy-start.5 = (f32[4,256,128]{2,1,0:T(8,128)S(1)}, f32[4,256,128]{2,1,0:T(8,128)}, u32[]{:S(2)}) copy-start(f32[4,256,128]{2,1,0:T(8,128)} %get-tuple-element.498) | copy-start | bytes 1572868 | tf_op jit(solution)/shard_map/while
  204.6 6.8 %copy-start.1 = (f32[4,2048,256]{2,1,0:T(8,128)S(1)}, f32[4,2048,256]{2,1,0:T(8,128)}, u32[]{:S(2)}) copy-start(f32[4,2048,256]{2,1,0:T(8,128)} %get-tuple-element.482) | copy-start | bytes 25165828 | tf_op jit(solution)/shard_map/while
  213.7 0.8 copy-start.6
  239.8 36.4 %copy-start.14 = (f32[4]{0:T(128)S(1)}, f32[4]{0:T(128)}, u32[]{:S(2)}) copy-start(f32[4]{0:T(128)} %param.32) | copy-start | bytes 52
  239.8 38.2 %copy-start.16 = (f32[128]{0:T(128)S(1)}, f32[128]{0:T(128)}, u32[]{:S(2)}) copy-start(f32[128]{0:T(128)} %param.33) | copy-start | bytes 1540
  248.2 6.8 %copy-start.3 = (f32[4,256,128]{2,1,0:T(8,128)S(1)}, f32[4,256,128]{2,1,0:T(8,128)}, u32[]{:S(2)}) copy-start(f32[4,256,128]{2,1,0:T(8,128)} %get-tuple-element.531) | copy-start | bytes 1572868 | tf_op jit(solution)/shard_map/while
  248.2 6.8 %copy-start.2 = (f32[4,2048,256]{2,1,0:T(8,128)S(1)}, f32[4,2048,256]{2,1,0:T(8,128)}, u32[]{:S(2)}) copy-start(f32[4,2048,256]{2,1,0:T(8,128)} %get-tuple-element.471) | copy-start | bytes 25165828 | tf_op jit(solution)/shard_map/while
  257.2 0.8 copy-start.4
  266.4 6.8 %copy-start.3 = (f32[4,256,128]{2,1,0:T(8,128)S(1)}, f32[4,256,128]{2,1,0:T(8,128)}, u32[]{:S(2)}) copy-start(f32[4,256,128]{2,1,0:T(8,128)} %get-tuple-element.531) | copy-start | bytes 1572868 | tf_op jit(solution)/shard_map/while
  266.4 6.8 %copy-start.2 = (f32[4,2048,256]{2,1,0:T(8,128)S(1)}, f32[4,2048,256]{2,1,0:T(8,128)}, u32[]{:S(2)}) copy-start(f32[4,2048,256]{2,1,0:T(8,128)} %get-tuple-element.471) | copy-start | bytes 25165828 | tf_op jit(solution)/shard_map/while
  275.4 0.8 copy-start.4
Sparse Core Ops, SparseCore 0:
  8.9 11.7 all-gather.4
  37.8 78.3 all-gather.8
  119.0 58.9 all-gather.10
  180.6 59.1 all-gather.6
  283.9 7.1 reduce-scatter.1
where the time goes:
time: 298 us
  waiting for transfers between devices  156 us (52%)
  local copies, waits for them, and re-layouts  53.4 us (18%)
  matrix products  42.4 us (14%)
  other arithmetic  25.1 us (8%)
  between operations  13.4 us (4%)
  starting transfers between devices  7.14 us (2%)
    all_gather x1, waiting for transfers between devices, local(): lax.all_gather(values, 'sp', axis=0, tiled=True)  66.4 us
    all_gather x1, waiting for transfers between devices, local(): lax.all_gather(second_key, 'sp', axis=0, tiled=True)  55.4 us
    all_gather x1, waiting for transfers between devices, local(): lax.all_gather(first_key, 'sp', axis=0, tiled=True)  25.3 us
    unnamed x31, local copies, waits for them, and re-layouts  23.4 us
    dynamic_slice x12, local copies, waits for them, and re-layouts, one_turn(): lax.dynamic_slice_in_dim(piece, index * size, size, 0)  22.4 us
    reduce_sum x4, other arithmetic, absorb(): totals = totals * factor + jnp.sum(weights, axis=2, keepdims=True)  19.7 us
    dot_general x4, matrix products, absorb(): jnp.einsum('qhd,khd->hqk', queries, keys, preferred_element_type=jnp.floa...  18.2 us
    dot_general x1, matrix products, local(): running = jnp.dot(scaled, stacked, preferred_element_type=jnp.float32)  9.46 us
  transfers between devices with their start and end apart: 7, of which 5 were waited for; matrix products, arithmetic and copies ran while one was open for 21% of the time, Pallas kernels for 0%

commit v1 on v0

v1 whole, which is shorter than its diff:
```python
import functools
import math

import jax
import jax.numpy as jnp
from jax import lax
from jax.experimental import pallas as pl
from jax.experimental.pallas import tpu as pltpu
from jax.sharding import PartitionSpec as P

EPSILON = 1e-06
MESH = pl.DeviceIdType.MESH
F32 = jnp.float32
BF16 = jnp.bfloat16
HALO = 16


def remote(src, dst, send_sem, recv_sem, sp, tp):
    return pltpu.make_async_remote_copy(
        src_ref=src,
        dst_ref=dst,
        send_sem=send_sem,
        recv_sem=recv_sem,
        device_id=(sp, tp),
        device_id_type=MESH,
    )


def kernel(
    S,
    T,
    H,
    KD,
    VD,
    tokens,
    gain,
    taps,
    head_gain,
    lam,
    w_k1,
    w_k2,
    w_v,
    w_q1,
    w_q2,
    w_ia,
    w_ib,
    w_outer,
    w_gate,
    w_ao,
    w_co,
    out,
    s_k1,
    s_k2,
    s_v,
    s_q1,
    s_q2,
    s_ia,
    s_ib,
    s_outer,
    s_gate,
    s_ao,
    s_co,
    tok,
    scaled,
    kv_send,
    kv_all,
    q_send,
    q_all,
    qz,
    acc,
    peak,
    total,
    prod,
    halo_lo,
    halo_hi,
    outer_y,
    gate_y,
    pre,
    att_out,
    att_in,
    mix,
    part_send,
    part_in,
    w_sem,
    tok_ss,
    tok_rs,
    kv_ss,
    kv_rs,
    fw_ss,
    q_ss,
    q_rs,
    halo_ss,
    halo_rs,
    att_ss,
    att_rs,
    part_ss,
    part_rs,
):
    G = S // H
    R, DT = tokens.shape
    D = DT * T
    me = lax.axis_index("sp")
    t = lax.axis_index("tp")
    h = me // G
    c = me % G

    hbm = (w_k1, w_k2, w_v, w_q1, w_q2, w_ia, w_ib, w_outer, w_gate, w_co, w_ao)
    vmem = (s_k1, s_k2, s_v, s_q1, s_q2, s_ia, s_ib, s_outer, s_gate, s_co, s_ao)
    loads = [pltpu.make_async_copy(a, b, w_sem.at[i]) for i, (a, b) in enumerate(zip(hbm, vmem))]
    for load in loads:
        load.start()
    ready = dict(zip([id(b) for b in vmem], loads))

    def tp_peer(k):
        return lax.rem(t + k, T)

    def head_peer(k):
        return lax.rem(h + k, H)

    def lane_peer(k):
        return lax.rem(c + k, G)

    lo = lax.rem(me + S - 1, S)
    hi = lax.rem(me + 1, S)

    barrier = pltpu.get_barrier_semaphore()
    greeted = 0
    for k in range(1, T):
        pl.semaphore_signal(barrier, inc=1, device_id=(me, tp_peer(k)), device_id_type=MESH)
        greeted += 1
    for k in range(1, H):
        pl.semaphore_signal(barrier, inc=1, device_id=(head_peer(k) * G + c, t), device_id_type=MESH)
        greeted += 1
    for k in range(1, G):
        pl.semaphore_signal(barrier, inc=1, device_id=(h * G + lane_peer(k), t), device_id_type=MESH)
        greeted += 1
    for other in (lo, hi):
        pl.semaphore_signal(barrier, inc=1, device_id=(other, t), device_id_type=MESH)
        greeted += 1
    pl.semaphore_wait(barrier, greeted)

    tok_copies = [
        remote(tokens, tok.at[t], tok_ss.at[k], tok_rs.at[k], me, tp_peer(k)) for k in range(1, T)
    ]
    for copy in tok_copies:
        copy.start()
    tok[t] = tokens[...]
    acc[...] = jnp.zeros_like(acc)
    peak[...] = jnp.full_like(peak, -1e30)
    total[...] = jnp.zeros_like(total)
    for copy in tok_copies:
        copy.wait()
    squares = jnp.zeros((R, 1), F32)
    for i in range(T):
        wide = tok[i].astype(F32)
        squares = squares + jnp.sum(wide * wide, axis=1, keepdims=True)
        scaled[:, i * DT : (i + 1) * DT] = (wide * gain[:, i * DT : (i + 1) * DT]).astype(BF16)
    inv = lax.rsqrt(squares / D + EPSILON)

    def project(w):
        ready[id(w)].wait()
        return jnp.dot(scaled[...], w[...], preferred_element_type=F32) * inv

    def halves(a, b, p):
        return jnp.concatenate(
            [a[:, p * KD : (p + 1) * KD], b[:, p * KD : (p + 1) * KD]], axis=1
        ).astype(BF16)

    k1 = project(s_k1)
    k2 = project(s_k2)
    for p in range(H):
        kv_send[p, :, : 2 * KD] = halves(k1, k2, p)
    values = project(s_v).astype(BF16)
    for p in range(H):
        kv_send[p, :, 2 * KD :] = values[:, p * VD : (p + 1) * VD]
    my_rows = pl.ds(pl.multiple_of(me * R, R), R)
    kv_copies = [
        remote(
            kv_send.at[head_peer(k)],
            kv_all.at[my_rows],
            kv_ss.at[k],
            kv_rs.at[me],
            head_peer(k) * G + c,
            t,
        )
        for k in range(1, H)
    ]
    for copy in kv_copies:
        copy.start()
    kv_all[my_rows] = kv_send[h]

    def arrival(source):
        rows = kv_all.at[pl.ds(pl.multiple_of(source * R, R), R)]
        return remote(rows, rows, fw_ss.at[0, 0], kv_rs.at[source], me, t)

    def forward(k, m):
        source = lax.rem(h + H - k, H) * G + c
        rows = kv_all.at[pl.ds(pl.multiple_of(source * R, R), R)]
        return remote(rows, rows, fw_ss.at[k, m], kv_rs.at[source], h * G + lane_peer(m), t)

    def forward_all(k):
        if k:
            arrival(lax.rem(h + H - k, H) * G + c).wait_recv()
        for m in range(1, G):
            forward(k, m).start()

    forward_all(0)

    q1 = project(s_q1)
    q2 = project(s_q2)
    for p in range(H):
        q_send[p] = halves(q1, q2, p)
    q_copies = [
        remote(
            q_send.at[head_peer(k)], q_all.at[h], q_ss.at[k], q_rs.at[h], head_peer(k) * G + c, t
        )
        for k in range(1, H)
    ]
    for copy in q_copies:
        copy.start()
    q_all[h] = q_send[h]

    inner_a = project(s_ia).astype(BF16).astype(F32)
    inner_b = project(s_ib).astype(BF16).astype(F32)
    prod[...] = (inner_a * inner_b).astype(BF16)
    halo_copies = [
        remote(prod.at[pl.ds(R - HALO, HALO)], halo_lo, halo_ss.at[0], halo_rs.at[0], hi, t),
        remote(prod.at[pl.ds(0, HALO)], halo_hi, halo_ss.at[1], halo_rs.at[1], lo, t),
    ]
    for copy in halo_copies:
        copy.start()
    if H > 1:
        forward_all(1)
    outer_y[...] = project(s_outer).astype(BF16)
    if H > 2:
        forward_all(2)
    gate_y[...] = project(s_gate).astype(BF16)
    for k in range(3, H):
        forward_all(k)

    for copy in halo_copies:
        copy.wait()
    wide = prod[...].astype(F32)
    row = lax.broadcasted_iota(jnp.int32, wide.shape, 0)
    first = jnp.where(me == 0, 0.0, halo_lo[...].astype(F32)[HALO - 1 : HALO])
    last = jnp.where(me == S - 1, 0.0, halo_hi[...].astype(F32)[0:1])
    before = jnp.where(row == 0, first, pltpu.roll(wide, 1, 0))
    after = jnp.where(row == R - 1, last, pltpu.roll(wide, R - 1, 0))
    tap = taps[...].astype(F32)
    convolved = tap[0:1] * before + tap[1:2] * wide + tap[2:3] * after
    conv_mix = (outer_y[...].astype(F32) * convolved).astype(BF16)
    ready[id(s_co)].wait()
    pre[...] = jnp.dot(conv_mix, s_co[...], preferred_element_type=F32)

    for k in range(1, H):
        source = lax.rem(h + H - k, H)
        remote(q_all.at[source], q_all.at[source], q_ss.at[k], q_rs.at[source], me, t).wait_recv()
    for p in range(H):
        both = q_all[p].astype(F32)
        lane = lax.broadcasted_iota(jnp.int32, both.shape, 1)
        qz[p, :R] = jnp.where(lane < KD, both, 0.0).astype(BF16)
        qz[p, R:] = jnp.where(lane < KD, 0.0, both).astype(BF16)

    group = G * R
    block = math.gcd(group, 1024)
    chunks = group // block
    factor = math.log2(math.e) / math.sqrt(KD)
    my_lam = lam[h]

    def finish(j, qi):
        state = acc[qi] / total[qi]
        diff = state[:R] - my_lam * state[R:]
        normed = diff * lax.rsqrt(jnp.mean(diff * diff, axis=1, keepdims=True) + EPSILON)
        att_out[qi] = (normed * head_gain[...]).astype(BF16)

        if H > 1:

            @pl.when(j < H - 1)
            def _():
                remote(
                    att_out.at[qi], att_in.at[h], att_ss.at[j], att_rs.at[h], qi * G + c, t
                ).start()

        @pl.when(j == H - 1)
        def _():
            att_in[h] = att_out[qi]

    def one_group(k, carry):
        source_head = lax.rem(h + H - k, H)
        for m in range(1, G):
            arrival(source_head * G + lane_peer(m)).wait_recv()

        def one_chunk(step, inner):
            ch = step // H
            j = lax.rem(step, H)
            qi = lax.rem(h + 1 + j, H)
            keys = pl.ds(pl.multiple_of(source_head * group + ch * block, block), block)
            scores = lax.dot_general(
                qz[qi],
                kv_all[keys, : 2 * KD],
                (((1,), (1,)), ((), ())),
                preferred_element_type=F32,
            )
            old = peak[qi]
            new = jnp.maximum(old, jnp.max(scores, axis=1, keepdims=True))
            weights = jnp.exp2((scores - new) * factor)
            scale = jnp.exp2((old - new) * factor)
            total[qi] = total[qi] * scale + jnp.sum(weights, axis=1, keepdims=True)
            acc[qi] = acc[qi] * scale + jnp.dot(
                weights.astype(BF16), kv_all[keys, 2 * KD :], preferred_element_type=F32
            )
            peak[qi] = new

            @pl.when((k == H - 1) & (ch == chunks - 1))
            def _():
                finish(j, qi)

            return inner

        lax.fori_loop(0, chunks * H, one_chunk, 0)
        return carry

    lax.fori_loop(0, H, one_group, 0)

    for k in range(1, H):
        source = lax.rem(h + H - k, H)
        remote(
            att_in.at[source], att_in.at[source], att_ss.at[0], att_rs.at[source], me, t
        ).wait_recv()
    for p in range(H):
        gate = gate_y[:, p * VD : (p + 1) * VD].astype(F32)
        mix[:, p * VD : (p + 1) * VD] = (
            att_in[p].astype(F32) * (gate / (1.0 + jnp.exp(-gate)))
        ).astype(BF16)
    ready[id(s_ao)].wait()
    RT = R // T

    def partial(owner):
        rows = pl.ds(pl.multiple_of(owner * RT, RT), RT)
        return (
            jnp.dot(mix[rows], s_ao[...], preferred_element_type=F32) + pre[rows]
        ).astype(BF16)

    part_copies = []
    for k in range(1, T):
        part_send[k - 1] = partial(tp_peer(k))
        copy = remote(
            part_send.at[k - 1], part_in.at[k - 1], part_ss.at[k], part_rs.at[k], me, tp_peer(k)
        )
        copy.start()
        part_copies.append(copy)
    mixed = partial(t).astype(F32)
    for k, copy in enumerate(part_copies):
        copy.wait()
        mixed = mixed + part_in[k].astype(F32)
    out[...] = mixed.astype(BF16)

    for copy in kv_copies + q_copies:
        copy.wait_send()
    for k in range(H):
        for m in range(1, G):
            forward(k, m).wait_send()
    for j in range(H - 1):
        qi = lax.rem(h + 1 + j, H)
        remote(att_out.at[qi], att_in.at[h], att_ss.at[j], att_rs.at[h], qi * G + c, t).wait_send()


def local(
    S,
    T,
    tokens,
    norm_gain,
    query_one,
    key_one,
    query_two,
    key_two,
    value_weight,
    attn_gate_weight,
    conv_outer,
    conv_inner,
    conv_input,
    conv_taps,
    head_lambda,
    head_gain,
    attn_out_weight,
    conv_out_weight,
):
    R, DT = tokens.shape
    D = DT * T
    H = head_lambda.shape[0]
    KD = key_one.shape[1] // H
    VD = value_weight.shape[1] // H
    C = conv_taps.shape[1]
    G = S // H
    RT = R // T
    weights = (
        key_one,
        key_two,
        value_weight,
        query_one,
        query_two,
        conv_inner,
        conv_input,
        conv_outer,
        attn_gate_weight,
        attn_out_weight,
        conv_out_weight,
    )
    vm = pl.BlockSpec(memory_space=pltpu.VMEM)
    dma = pltpu.SemaphoreType.DMA
    return pl.pallas_call(
        functools.partial(kernel, S, T, H, KD, VD),
        out_shape=jax.ShapeDtypeStruct((RT, D), BF16),
        in_specs=[vm] * 4
        + [pl.BlockSpec(memory_space=pltpu.SMEM)]
        + [pl.BlockSpec(memory_space=pl.ANY)] * len(weights),
        out_specs=vm,
        scratch_shapes=[pltpu.VMEM(w.shape, BF16) for w in weights]
        + [
            pltpu.VMEM((T, R, DT), BF16),
            pltpu.VMEM((R, D), BF16),
            pltpu.VMEM((H, R, 2 * KD + VD), BF16),
            pltpu.VMEM((S * R, 2 * KD + VD), BF16),
            pltpu.VMEM((H, R, 2 * KD), BF16),
            pltpu.VMEM((H, R, 2 * KD), BF16),
            pltpu.VMEM((H, 2 * R, 2 * KD), BF16),
            pltpu.VMEM((H, 2 * R, VD), F32),
            pltpu.VMEM((H, 2 * R, 1), F32),
            pltpu.VMEM((H, 2 * R, 1), F32),
            pltpu.VMEM((R, C), BF16),
            pltpu.VMEM((HALO, C), BF16),
            pltpu.VMEM((HALO, C), BF16),
            pltpu.VMEM((R, C), BF16),
            pltpu.VMEM((R, H * VD), BF16),
            pltpu.VMEM((R, D), F32),
            pltpu.VMEM((H, R, VD), BF16),
            pltpu.VMEM((H, R, VD), BF16),
            pltpu.VMEM((R, H * VD), BF16),
            pltpu.VMEM((max(T - 1, 1), RT, D), BF16),
            pltpu.VMEM((max(T - 1, 1), RT, D), BF16),
            dma((len(weights),)),
            dma((T,)),
            dma((T,)),
            dma((H,)),
            dma((S,)),
            dma((H, G)),
            dma((H,)),
            dma((H,)),
            dma((2,)),
            dma((2,)),
            dma((H,)),
            dma((H,)),
            dma((T,)),
            dma((T,)),
        ],
        compiler_params=pltpu.CompilerParams(
            collective_id=0, has_side_effects=True, vmem_limit_bytes=60 * 1024 * 1024
        ),
        name="layer",
    )(
        tokens,
        norm_gain.reshape(1, D),
        conv_taps,
        head_gain.reshape(1, VD),
        head_lambda,
        *weights,
    )


def solution(mesh):
    S = mesh.shape["sp"]
    T = mesh.shape["tp"]
    return jax.shard_map(
        functools.partial(local, S, T),
        mesh=mesh,
        in_specs=(P("sp", "tp"), P())
        + (P(None, "tp"),) * 10
        + (P("tp"), P(), P("tp", None), P("tp", None)),
        out_specs=P(("sp", "tp"), None),
        check_vma=False,
    )
```

time: 298 us -> 67.2 us (0.23)
  waiting for transfers between devices: 156 us -> 0 us
  Pallas kernels: 0 us -> 65.1 us
  local copies, waits for them, and re-layouts: 53.4 us -> 1.88 us
  matrix products: 42.4 us -> 0 us
  other arithmetic: 25.1 us -> 0 us
  between operations: 13.4 us -> 0.01 us
  starting transfers between devices: 7.14 us -> 0 us
    all_gather x4 -> x0, waiting for transfers between devices: 147 us -> none  [the longest x1 66.4 us: local(): lax.all_gather(values, 'sp', axis=0, tiled=True)]
    pallas_call x0 -> x1, Pallas kernels: none -> 65.1 us  [local(): pl.pallas_call(functools.partial(kernel, S, T, H, KD, VD), out_shape=jax....]
    dot_general x11 -> x0, matrix products: 42.4 us -> none  [the longest x4 18.2 us: absorb(): jnp.einsum('qhd,khd->hqk', queries, keys, preferred_element_type=jnp.floa...]
    reduce_sum x6 -> x0, other arithmetic: 23 us -> none  [the longest x4 19.7 us: absorb(): totals = totals * factor + jnp.sum(weights, axis=2, keepdims=True)]
    dynamic_slice x12 -> x0, local copies, waits for them, and re-layouts: 22.4 us -> none  [one_turn(): lax.dynamic_slice_in_dim(piece, index * size, size, 0)]
    unnamed x31 -> x1, local copies, waits for them, and re-layouts: 23.4 us -> 1.88 us
    reduce_scatter x1 -> x0, waiting for transfers between devices: 7.35 us -> none  [local(): lax.psum_scatter((jnp.dot(attn_mix, attn_out_weight, preferred_element_ty...]
    ppermute x2 -> x0, starting transfers between devices: 6.79 us -> none  [the longest x1 5.5 us: with_halo(): lax.ppermute(tail, axis, [(i, (i + 1) % count) for i in range(ends)])]
  transfers between devices with their start and end apart: 7 -> 0, of which waited for: 5 -> 0; matrix products, arithmetic and copies ran while one was open for 21% -> 0% of each run, Pallas kernels for 0% -> 0%
where the time goes in v1:
time: 67.2 us; the launch traced here: 67 us
  Pallas kernels  65.1 us (97%)
  local copies, waits for them, and re-layouts  1.88 us (3%)
    pallas_call x1, Pallas kernels, local(): pl.pallas_call(functools.partial(kernel, S, T, H, KD, VD), out_shape=jax....  65.1 us
    unnamed x1, local copies, waits for them, and re-layouts  1.88 us

profile of v1, /device:TPU:0, one launch (start us, length us, event | category | flops | bytes accessed | tf_op | source)
XLA Modules:
  0.0 67.0 jit_solution(6076692192572957564)
XLA Ops:
  0.0 65.1 %layer.1 = bf16[128,2048]{1,0:T(8,128)(2,1)} custom-call(bf16[256,1024]{1,0:T(8,128)(2,1)} %tokens.1, f32[1,2048]{1,0:T(1,128)} %bitcast.2, bf16[3,512]{1,0:T(4,128)(2,1)} %taps.1, f32[1,128]{1,0:T(1,128)} %bitcast.3, f32[4]{0:T(128)} %lam.1, bf16[2048,256]{1,0:T(8,128)(2,1)} %w_k1.1, bf16[2048,256]{1,0:T(8,128)(2,1)} %w_k2.1, bf16[2048,512]{1,0:T(8,128)(2,1)} %w_v.1, ...), custom_call_target="tpu_custom_call" | custom-call | tf_op jit(solution)/shard_map/layer/pallas_call | solution.py:411
  65.1 1.9 %copy.18 = bf16[128,2048]{1,0:T(8,128)(2,1)} copy(bf16[128,2048]{1,0:T(8,128)(2,1)} %layer.1) | data formatting | bytes 1048576

commit v2 on v1

--- a/solution.py
+++ b/solution.py
@@ -13,6 +13,7 @@
 F32 = jnp.float32
 BF16 = jnp.bfloat16
 HALO = 16
+TILES = 4
 
 
 def remote(src, dst, send_sem, recv_sem, sp, tp):
@@ -199,7 +200,7 @@
         return remote(rows, rows, fw_ss.at[k, m], kv_rs.at[source], h * G + lane_peer(m), t)
 
     def forward_all(k):
-        if k:
+        if not (isinstance(k, int) and k == 0):
             arrival(lax.rem(h + H - k, H) * G + c).wait_recv()
         for m in range(1, G):
             forward(k, m).start()
@@ -235,6 +236,7 @@
     if H > 2:
         forward_all(2)
     gate_y[...] = project(s_gate).astype(BF16)
+
     for k in range(3, H):
         forward_all(k)
 
@@ -295,21 +297,45 @@
             j = lax.rem(step, H)
             qi = lax.rem(h + 1 + j, H)
             keys = pl.ds(pl.multiple_of(source_head * group + ch * block, block), block)
-            scores = lax.dot_general(
-                qz[qi],
-                kv_all[keys, : 2 * KD],
-                (((1,), (1,)), ((), ())),
-                preferred_element_type=F32,
-            )
-            old = peak[qi]
-            new = jnp.maximum(old, jnp.max(scores, axis=1, keepdims=True))
-            weights = jnp.exp2((scores - new) * factor)
-            scale = jnp.exp2((old - new) * factor)
-            total[qi] = total[qi] * scale + jnp.sum(weights, axis=1, keepdims=True)
-            acc[qi] = acc[qi] * scale + jnp.dot(
-                weights.astype(BF16), kv_all[keys, 2 * KD :], preferred_element_type=F32
-            )
-            peak[qi] = new
+            keys_ref = kv_all[keys, : 2 * KD]
+            vals_ref = kv_all[keys, 2 * KD :]
+            tile = 2 * R // TILES
+
+            def score(i):
+                return lax.dot_general(
+                    qz[qi, i * tile : (i + 1) * tile],
+                    keys_ref,
+                    (((1,), (1,)), ((), ())),
+                    preferred_element_type=F32,
+                )
+
+            def soften(i, scores):
+                rows = slice(i * tile, (i + 1) * tile)
+                old = peak[qi, rows]
+                new = jnp.maximum(old, jnp.max(scores, axis=1, keepdims=True))
+                spread = jnp.concatenate([new] * (block // new.shape[1]), axis=1)
+                weights = jnp.exp2((scores - spread) * factor)
+                scale = jnp.exp2((old - new) * factor)
+                total[qi, rows] = total[qi, rows] * scale + jnp.sum(weights, axis=1, keepdims=True)
+                peak[qi, rows] = new
+                return weights.astype(BF16), scale
+
+            def gather(i, weights, scale):
+                rows = slice(i * tile, (i + 1) * tile)
+                acc[qi, rows] = acc[qi, rows] * scale + jnp.dot(
+                    weights, vals_ref, preferred_element_type=F32
+                )
+
+            ahead = score(0)
+            held = None
+            for i in range(TILES):
+                current = ahead
+                if i + 1 < TILES:
+                    ahead = score(i + 1)
+                if held is not None:
+                    gather(i - 1, *held)
+                held = soften(i, current)
+            gather(TILES - 1, *held)
 
             @pl.when((k == H - 1) & (ch == chunks - 1))
             def _():
@@ -425,8 +451,8 @@
             pltpu.VMEM((H, R, 2 * KD), BF16),
             pltpu.VMEM((H, 2 * R, 2 * KD), BF16),
             pltpu.VMEM((H, 2 * R, VD), F32),
-            pltpu.VMEM((H, 2 * R, 1), F32),
-            pltpu.VMEM((H, 2 * R, 1), F32),
+            pltpu.VMEM((H, 2 * R, VD), F32),
+            pltpu.VMEM((H, 2 * R, VD), F32),
             pltpu.VMEM((R, C), BF16),
             pltpu.VMEM((HALO, C), BF16),
             pltpu.VMEM((HALO, C), BF16),

time: 67.2 us -> 56.7 us (0.84)
  Pallas kernels: 65.1 us -> 54.7 us
    pallas_call x1, Pallas kernels: 65.1 us -> 54.7 us  [local(): pl.pallas_call(functools.partial(kernel, S, T, H, KD, VD), out_shape=jax....]
where the time goes in v2:
time: 56.7 us; the launch traced here: 56.6 us
  Pallas kernels  54.7 us (96%)
  local copies, waits for them, and re-layouts  1.88 us (3%)
    pallas_call x1, Pallas kernels, local(): pl.pallas_call(functools.partial(kernel, S, T, H, KD, VD), out_shape=jax....  54.7 us
    unnamed x1, local copies, waits for them, and re-layouts  1.88 us

profile of v2, /device:TPU:0, one launch (start us, length us, event | category | flops | bytes accessed | tf_op | source)
XLA Modules:
  0.0 56.6 jit_solution(157758622876037987)
XLA Ops:
  0.0 54.7 %layer.1 = bf16[128,2048]{1,0:T(8,128)(2,1)} custom-call(bf16[256,1024]{1,0:T(8,128)(2,1)} %tokens.1, f32[1,2048]{1,0:T(1,128)} %bitcast.2, bf16[3,512]{1,0:T(4,128)(2,1)} %taps.1, f32[1,128]{1,0:T(1,128)} %bitcast.3, f32[4]{0:T(128)} %lam.1, bf16[2048,256]{1,0:T(8,128)(2,1)} %w_k1.1, bf16[2048,256]{1,0:T(8,128)(2,1)} %w_k2.1, bf16[2048,512]{1,0:T(8,128)(2,1)} %w_v.1, ...), custom_call_target="tpu_custom_call" | custom-call | tf_op jit(solution)/shard_map/layer/pallas_call | solution.py:437
  54.7 1.9 %copy.18 = bf16[128,2048]{1,0:T(8,128)(2,1)} copy(bf16[128,2048]{1,0:T(8,128)(2,1)} %layer.1) | data formatting | bytes 1048576
